TPU v7x, 32 devices: a whole 2x2x4 slice. The times are simulated.
32 devices in a mesh: sp: 8 (over z, y), tp: 4 (over x, core).
Axes of the slice: x: 2, y: 2, z: 4, core: 2. Of those that a mesh axis runs over, the one named last changes fastest.
Arguments:
- query: bfloat16 [2048, 1024], P('sp', 'tp'), may hold values from -12 to 12
- key_rows: bfloat16 [2048, 512], P('sp', 'tp'), may hold values from -8 to 8
- value_rows: bfloat16 [2048, 512], P('sp', 'tp'), may hold values from -16 to 16
- stream: bfloat16 [2048, 2048], P(('sp', 'tp')), may hold values from -6 to 6
- out_weight: bfloat16 [1024, 2048], P('tp'), may hold values from -0.1875 to 0.1875
- norm_gain: float32 [2048], replicated, may hold values from 0.1 to 1.9
- route_ids: int32 [2048, 4], P(('sp', 'tp')), may hold values from 0 to 7, all different within a row; in each aligned block of 64 rows (0 to 63, 64 to 127, ...) at most 64 rows name the same one
- route_weights: float32 [2048, 4], P(('sp', 'tp')), may hold values from 0.1 to 1
- expert_gate: bfloat16 [8, 2048, 384], P('sp'), may hold values from -0.125 to 0.125
- expert_up: bfloat16 [8, 2048, 384], P('sp'), may hold values from -0.125 to 0.125
- expert_down: bfloat16 [8, 384, 2048], P('sp'), may hold values from -0.3125 to 0.3125
- shared_gate: bfloat16 [2048, 384], replicated, may hold values from -0.125 to 0.125
- shared_up: bfloat16 [2048, 384], replicated, may hold values from -0.125 to 0.125
- shared_down: bfloat16 [384, 2048], replicated, may hold values from -0.3125 to 0.3125
Outputs:
- result: bfloat16 [2048, 2048], P(('sp', 'tp'))
Inputs may be any that keep to these rules, and one draw needn't show every extreme that they name: `route_ids`: each row names 4 different experts. Within the rows of one device (aligned blocks of 64 rows) no expert is named more than 64 times, and in some blocks one expert is named exactly 64 times.
All inputs are finite; a program needn't handle non-finite values.
Results may differ from a plain program's by a relative error of at most 0.007.
Values may be sent and summed in bfloat16 or wider, within the bound.
A program may use at most 128 MiB of HBM per device.

v0:
```python
import math

import jax
import jax.numpy as jnp
from jax import lax
from jax.sharding import PartitionSpec as P

D = 2048
HD = 128
TOP_K = 4
KB = 128


def shifted(value, axis, steps):
    count = lax.axis_size(axis)
    first, last = (max(0, -steps), min(count, count - steps))
    return lax.ppermute(value, axis, [(source, source + steps) for source in range(first, last)])


def soft_plus(values):
    return jnp.maximum(values, 0.0) + jnp.log1p(jnp.exp(-jnp.abs(values)))


def shard_scores(queries, shard_keys, shard_start, query_pos):
    key_count = shard_keys.shape[0]
    keys_split = shard_keys.reshape(key_count, queries.shape[1], queries.shape[3])
    logits = jnp.einsum("tkgd,skd->kgts", queries, keys_split, preferred_element_type=jnp.float32)
    logits = logits * (1.0 / math.sqrt(queries.shape[3]))
    key_pos = shard_start + jnp.arange(key_count, dtype=jnp.int32)
    visible = key_pos[None, :] < query_pos[:, None]
    penalty = soft_plus(logits)
    breaks = jnp.where(visible, -penalty, 0.0)
    return (logits, penalty, breaks, visible)


def grouped(values, block_size):
    full_shape = values.shape
    return values.reshape(full_shape[:-1] + (full_shape[-1] // block_size, block_size))


def later_matrix(length):
    positions = jnp.arange(length)
    return (positions[:, None] > positions[None, :]).astype(jnp.float32)


def later_sum(values, length):
    return jnp.einsum(
        "kgtm,mb->kgtb", values, later_matrix(length), precision=lax.Precision.HIGHEST
    )


def stick_weights(logits, penalty, breaks, visible, carried, block_size):
    inside = jnp.einsum(
        "kgtnj,js->kgtns",
        grouped(breaks, block_size),
        later_matrix(block_size),
        precision=lax.Precision.HIGHEST,
    )
    log_weight = (
        logits - penalty + inside.reshape(breaks.shape) + jnp.repeat(carried, block_size, axis=3)
    )
    return jnp.where(visible, jnp.exp(log_weight), 0.0).astype(jnp.bfloat16)


def add_values(running, weights, shard_values):
    values_split = shard_values.reshape(shard_values.shape[0], running.shape[0], running.shape[3])
    return running + jnp.einsum(
        "kgts,skd->kgtd", weights, values_split, preferred_element_type=jnp.float32
    )


def keep_state(current_state):
    return current_state


def per_device(
    query,
    key_rows,
    value_rows,
    stream,
    out_weight,
    norm_gain,
    route_ids,
    route_weights,
    expert_gate,
    expert_up,
    expert_down,
    shared_gate,
    shared_up,
    shared_down,
):
    tok_rows = query.shape[0]
    kv_local = key_rows.shape[1] // HD
    group_size = query.shape[1] // key_rows.shape[1]
    queries = query.reshape(tok_rows, kv_local, group_size, HD)
    device_pos = lax.axis_index("sp")
    offset = device_pos * tok_rows
    query_pos = offset + jnp.arange(tok_rows, dtype=jnp.int32)
    shard_blocks = tok_rows // KB
    zero_mixed = jnp.zeros((kv_local, group_size, tok_rows, HD), jnp.float32)

    def chain_visit(current_state, shard_keys, shard_values, shard_start):
        mixed_sums, carried_total = current_state
        logits, penalty, breaks, visible = shard_scores(queries, shard_keys, shard_start, query_pos)
        block_totals = grouped(breaks, KB).sum(axis=4)
        carried = later_sum(block_totals, shard_blocks) + carried_total[..., None]
        weights = stick_weights(logits, penalty, breaks, visible, carried, KB)
        return (
            add_values(mixed_sums, weights, shard_values),
            carried_total + block_totals.sum(axis=3),
        )

    start_state = chain_visit(
        (zero_mixed, jnp.zeros((kv_local, group_size, tok_rows), jnp.float32)),
        key_rows,
        value_rows,
        offset,
    )
    moving = jnp.stack((key_rows, value_rows))

    def turn(distance, loop_state):
        current, travelling = loop_state
        travelling = shifted(travelling, "sp", 1)

        def evaluate_layer(current_state):
            return chain_visit(
                current_state, travelling[0], travelling[1], offset - distance * tok_rows
            )

        current = lax.cond(distance <= device_pos, evaluate_layer, keep_state, current)
        return (current, travelling)

    mixed_sums = lax.fori_loop(1, lax.axis_size("sp"), turn, (start_state, moving))[0][0]
    heads_out = (
        mixed_sums.astype(jnp.bfloat16)
        .transpose(2, 0, 1, 3)
        .reshape(tok_rows, kv_local * group_size * HD)
    )
    own_rows = stream.shape[0]
    attended = lax.psum_scatter(
        jnp.dot(heads_out, out_weight, preferred_element_type=jnp.float32),
        "tp",
        scatter_dimension=0,
        tiled=True,
    )
    mid = (stream.astype(jnp.float32) + attended).astype(jnp.bfloat16)
    mid_wide = lax.optimization_barrier(mid).astype(jnp.float32)
    normed = (
        mid_wide
        * lax.rsqrt(jnp.mean(mid_wide * mid_wide, axis=1, keepdims=True) + 1e-06)
        * norm_gain
    ).astype(jnp.bfloat16)
    local_experts = expert_gate.shape[0]
    expert_count = lax.axis_size("sp") * local_experts
    capacity = 2 * own_rows * TOP_K // expert_count
    slot_count = expert_count * capacity
    flat_ids = route_ids.reshape(-1)
    membership = (flat_ids[:, None] == jnp.arange(expert_count, dtype=jnp.int32)[None, :]).astype(
        jnp.int32
    )
    before = jnp.cumsum(membership, axis=0) - membership
    slot_rank = jnp.sum(before * membership, axis=1)
    slot_ids = flat_ids * capacity + slot_rank
    placing = jnp.arange(slot_count, dtype=jnp.int32)[:, None] == slot_ids[None, :]
    dispatch = placing.reshape(slot_count, own_rows, TOP_K).any(axis=2).astype(jnp.bfloat16)
    outgoing = jnp.dot(dispatch, normed, preferred_element_type=jnp.float32).astype(jnp.bfloat16)
    outgoing = outgoing.reshape(lax.axis_size("sp"), local_experts, capacity, D)
    arrived = lax.all_to_all(outgoing, "sp", split_axis=0, concat_axis=0, tiled=True)
    gate_part = jnp.einsum(
        "sepd,edf->sepf", arrived, expert_gate, preferred_element_type=jnp.float32
    )
    up_part = jnp.einsum("sepd,edf->sepf", arrived, expert_up, preferred_element_type=jnp.float32)
    hidden = (jax.nn.silu(gate_part) * up_part).astype(jnp.bfloat16)
    produced = jnp.einsum(
        "sepf,efd->sepd", hidden, expert_down, preferred_element_type=jnp.float32
    ).astype(jnp.bfloat16)
    returned = lax.all_to_all(produced, "sp", split_axis=0, concat_axis=0, tiled=True)
    returned = returned.reshape(slot_count, D)
    picking = (slot_ids[:, None] == jnp.arange(slot_count, dtype=jnp.int32)[None, :]).astype(
        jnp.bfloat16
    )
    selected_experts = jnp.dot(picking, returned, preferred_element_type=jnp.float32).reshape(
        own_rows, TOP_K, D
    )
    routed = jnp.sum(selected_experts * route_weights[:, :, None], axis=1)
    shared_hidden = (
        jax.nn.silu(jnp.dot(normed, shared_gate, preferred_element_type=jnp.float32))
        * jnp.dot(normed, shared_up, preferred_element_type=jnp.float32)
    ).astype(jnp.bfloat16)
    shared_out = jnp.dot(shared_hidden, shared_down, preferred_element_type=jnp.float32)
    return (mid_wide + routed + shared_out).astype(jnp.bfloat16)


def solution(mesh):
    in_specs = (
        P("sp", "tp"),
        P("sp", "tp"),
        P("sp", "tp"),
        P(("sp", "tp"), None),
        P("tp", None),
        P(),
        P(("sp", "tp"), None),
        P(("sp", "tp"), None),
        P("sp", None, None),
        P("sp", None, None),
        P("sp", None, None),
        P(),
        P(),
        P(),
    )
    out_specs = P(("sp", "tp"), None)
    return jax.shard_map(
        per_device, mesh=mesh, in_specs=in_specs, out_specs=out_specs, check_vma=False
    )
```

profile of v0, /device:TPU:0, one launch (start us, length us, event | category | flops | bytes accessed | tf_op | source)
XLA Modules:
  0.0 243.3 jit_solution(18195276336152702490)
XLA Ops:
  6.5 0.1 broadcast_compare_fusion.1
  6.7 1.1 copy.70
  7.8 1.5 fusion.102
  9.2 0.4 fusion.83
  9.7 0.1 fusion.94
  9.8 0.1 copy.71
  10.0 0.4 fusion.66
  10.4 0.3 convolution_bitcast_fusion.1
  10.7 57.4 %while.19 = (s32[]{:T(128)}, f32[1,2,256,128]{3,2,1,0:T(8,128)S(1)}, f32[1,2,256]{2,1,0:T(2,128)S(1)}, bf16[2,256,128]{2,1,0:T(8,128)(2,1)S(1)}, s32[]{:T(128)},...) while((s32[]{:T(128)}, f32[1,2,256,128]{3,2,1,0:T(8,128)S(1)}, ...), condition=%wide.region_7.8_spmd.clone.clone, body=%wide.region_2.7_spmd.clone.clone.sunk | while | flops 270967296 | bytes 5996823 | solution.py:133
  10.7 4.9 %collective-permute-start = (bf16[2,256,128]{2,1,0:T(8,128)(2,1)S(1)}, bf16[2,256,128]{2,1,0:T(8,128)(2,1)S(1)}, u32[]{:S(2)}, u32[]{:S(2)}) collective-permute-start(bf16[2,256,128]{2,1,0:T(8,128)(2,1)S(1)} %get-tuple-element.332), channel_id=1, source_target_pairs={{0,4},{4,8},{8,12},{12,16},{16,20},{20,24},{24,28},{1,5},{5,9},{9,... | collective-permute-start | bytes 393224 | tf_op jit(solution)/shard_map/while/body/eval_jaxpr/ppermute | solution.py:17
  15.6 2.7 %collective-permute-done = bf16[2,256,128]{2,1,0:T(8,128)(2,1)S(1)} collective-permute-done((bf16[2,256,128]{2,1,0:T(8,128)(2,1)S(1)}, bf16[2,256,128]{2,1,0:T(8,128)(2,1)S(1)}, u32[]{:S(2)}, u32[]{:S(2)}) %collective-permute-start) | collective-permute-done | bytes 131104 | tf_op jit(solution)/shard_map/while/body/eval_jaxpr/ppermute | solution.py:17
  18.3 6.3 %collective-permute-start = (bf16[2,256,128]{2,1,0:T(8,128)(2,1)S(1)}, bf16[2,256,128]{2,1,0:T(8,128)(2,1)S(1)}, u32[]{:S(2)}, u32[]{:S(2)}) collective-permute-start(bf16[2,256,128]{2,1,0:T(8,128)(2,1)S(1)} %get-tuple-element.332), channel_id=1, source_target_pairs={{0,4},{4,8},{8,12},{12,16},{16,20},{20,24},{24,28},{1,5},{5,9},{9,... | collective-permute-start | bytes 393224 | tf_op jit(solution)/shard_map/while/body/eval_jaxpr/ppermute | solution.py:17
  24.7 2.5 %collective-permute-done = bf16[2,256,128]{2,1,0:T(8,128)(2,1)S(1)} collective-permute-done((bf16[2,256,128]{2,1,0:T(8,128)(2,1)S(1)}, bf16[2,256,128]{2,1,0:T(8,128)(2,1)S(1)}, u32[]{:S(2)}, u32[]{:S(2)}) %collective-permute-start) | collective-permute-done | bytes 131104 | tf_op jit(solution)/shard_map/while/body/eval_jaxpr/ppermute | solution.py:17
  27.2 4.4 %collective-permute-start = (bf16[2,256,128]{2,1,0:T(8,128)(2,1)S(1)}, bf16[2,256,128]{2,1,0:T(8,128)(2,1)S(1)}, u32[]{:S(2)}, u32[]{:S(2)}) collective-permute-start(bf16[2,256,128]{2,1,0:T(8,128)(2,1)S(1)} %get-tuple-element.332), channel_id=1, source_target_pairs={{0,4},{4,8},{8,12},{12,16},{16,20},{20,24},{24,28},{1,5},{5,9},{9,... | collective-permute-start | bytes 393224 | tf_op jit(solution)/shard_map/while/body/eval_jaxpr/ppermute | solution.py:17
  31.6 2.5 %collective-permute-done = bf16[2,256,128]{2,1,0:T(8,128)(2,1)S(1)} collective-permute-done((bf16[2,256,128]{2,1,0:T(8,128)(2,1)S(1)}, bf16[2,256,128]{2,1,0:T(8,128)(2,1)S(1)}, u32[]{:S(2)}, u32[]{:S(2)}) %collective-permute-start) | collective-permute-done | bytes 131104 | tf_op jit(solution)/shard_map/while/body/eval_jaxpr/ppermute | solution.py:17
  34.1 7.2 %collective-permute-start = (bf16[2,256,128]{2,1,0:T(8,128)(2,1)S(1)}, bf16[2,256,128]{2,1,0:T(8,128)(2,1)S(1)}, u32[]{:S(2)}, u32[]{:S(2)}) collective-permute-start(bf16[2,256,128]{2,1,0:T(8,128)(2,1)S(1)} %get-tuple-element.332), channel_id=1, source_target_pairs={{0,4},{4,8},{8,12},{12,16},{16,20},{20,24},{24,28},{1,5},{5,9},{9,... | collective-permute-start | bytes 393224 | tf_op jit(solution)/shard_map/while/body/eval_jaxpr/ppermute | solution.py:17
  41.3 2.5 %collective-permute-done = bf16[2,256,128]{2,1,0:T(8,128)(2,1)S(1)} collective-permute-done((bf16[2,256,128]{2,1,0:T(8,128)(2,1)S(1)}, bf16[2,256,128]{2,1,0:T(8,128)(2,1)S(1)}, u32[]{:S(2)}, u32[]{:S(2)}) %collective-permute-start) | collective-permute-done | bytes 131104 | tf_op jit(solution)/shard_map/while/body/eval_jaxpr/ppermute | solution.py:17
  43.8 5.3 %collective-permute-start = (bf16[2,256,128]{2,1,0:T(8,128)(2,1)S(1)}, bf16[2,256,128]{2,1,0:T(8,128)(2,1)S(1)}, u32[]{:S(2)}, u32[]{:S(2)}) collective-permute-start(bf16[2,256,128]{2,1,0:T(8,128)(2,1)S(1)} %get-tuple-element.332), channel_id=1, source_target_pairs={{0,4},{4,8},{8,12},{12,16},{16,20},{20,24},{24,28},{1,5},{5,9},{9,... | collective-permute-start | bytes 393224 | tf_op jit(solution)/shard_map/while/body/eval_jaxpr/ppermute | solution.py:17
  49.1 2.5 %collective-permute-done = bf16[2,256,128]{2,1,0:T(8,128)(2,1)S(1)} collective-permute-done((bf16[2,256,128]{2,1,0:T(8,128)(2,1)S(1)}, bf16[2,256,128]{2,1,0:T(8,128)(2,1)S(1)}, u32[]{:S(2)}, u32[]{:S(2)}) %collective-permute-start) | collective-permute-done | bytes 131104 | tf_op jit(solution)/shard_map/while/body/eval_jaxpr/ppermute | solution.py:17
  51.6 5.4 %collective-permute-start = (bf16[2,256,128]{2,1,0:T(8,128)(2,1)S(1)}, bf16[2,256,128]{2,1,0:T(8,128)(2,1)S(1)}, u32[]{:S(2)}, u32[]{:S(2)}) collective-permute-start(bf16[2,256,128]{2,1,0:T(8,128)(2,1)S(1)} %get-tuple-element.332), channel_id=1, source_target_pairs={{0,4},{4,8},{8,12},{12,16},{16,20},{20,24},{24,28},{1,5},{5,9},{9,... | collective-permute-start | bytes 393224 | tf_op jit(solution)/shard_map/while/body/eval_jaxpr/ppermute | solution.py:17
  57.0 3.5 %collective-permute-done = bf16[2,256,128]{2,1,0:T(8,128)(2,1)S(1)} collective-permute-done((bf16[2,256,128]{2,1,0:T(8,128)(2,1)S(1)}, bf16[2,256,128]{2,1,0:T(8,128)(2,1)S(1)}, u32[]{:S(2)}, u32[]{:S(2)}) %collective-permute-start) | collective-permute-done | bytes 131104 | tf_op jit(solution)/shard_map/while/body/eval_jaxpr/ppermute | solution.py:17
  60.5 5.0 %collective-permute-start = (bf16[2,256,128]{2,1,0:T(8,128)(2,1)S(1)}, bf16[2,256,128]{2,1,0:T(8,128)(2,1)S(1)}, u32[]{:S(2)}, u32[]{:S(2)}) collective-permute-start(bf16[2,256,128]{2,1,0:T(8,128)(2,1)S(1)} %get-tuple-element.332), channel_id=1, source_target_pairs={{0,4},{4,8},{8,12},{12,16},{16,20},{20,24},{24,28},{1,5},{5,9},{9,... | collective-permute-start | bytes 393224 | tf_op jit(solution)/shard_map/while/body/eval_jaxpr/ppermute | solution.py:17
  65.6 2.5 %collective-permute-done = bf16[2,256,128]{2,1,0:T(8,128)(2,1)S(1)} collective-permute-done((bf16[2,256,128]{2,1,0:T(8,128)(2,1)S(1)}, bf16[2,256,128]{2,1,0:T(8,128)(2,1)S(1)}, u32[]{:S(2)}, u32[]{:S(2)}) %collective-permute-start) | collective-permute-done | bytes 131104 | tf_op jit(solution)/shard_map/while/body/eval_jaxpr/ppermute | solution.py:17
  68.1 0.1 copy.72
  68.2 3.0 %fusion.103 = f32[256,2048]{1,0:T(8,128)} fusion(bf16[256,256]{0,1:T(8,128)(2,1)S(1)} %bitcast.210, bf16[256,2048]{1,0:T(8,128)(2,1)} %param.22), kind=kOutput, calls=%fused_computation.110 | convolution fusion | flops 268435456 | bytes 3276800 | tf_op jit(solution)/shard_map/dot_general | solution.py:141
  71.2 0.7 copy-done.8
  71.9 0.1 copy.73
  72.0 0.1 eq.72
  72.1 0.1 eq.68
  72.2 0.6 reduce-window.6
  72.8 0.2 slice_reduce_fusion
  73.1 0.1 fusion.92
  73.2 0.1 reduce_sum.73
  73.3 0.1 copy.75
  73.4 0.2 fusion.69
  73.5 40.2 %reduce-scatter.2.cloned.1.call-done = f32[64,2048]{1,0:T(8,128)} async-done(((f32[256,2048]{1,0:T(8,128)}), f32[64,2048]{1,0:T(8,128)}) %reduce-scatter.2.cloned.1.call-update) | async-done | bytes 524304 | tf_op jit(solution)/shard_map/reduce_scatter | solution.py:140
  113.8 1.1 add_convert_fusion
  114.8 0.2 fusion.61
  115.0 0.8 convolution_convert_fusion.1
  115.8 53.5 %all_to_all.10 = bf16[8,1,64,2048]{3,2,1,0:T(8,128)(2,1)S(1)} all-to-all(bf16[8,1,64,2048]{3,2,1,0:T(8,128)(2,1)S(1)} %bitcast.207), channel_id=1, replica_groups=mesh['sp'=8,'tp'=4] {'sp'}, dimensions={0} | all-to-all | bytes 4194304 | tf_op jit(solution)/shard_map/all_to_all | solution.py:168
  169.4 1.3 copy-done.1
  170.7 2.1 fusion.30
  172.8 5.5 %fusion.20 = bf16[8,1,64,2048]{3,2,1,0:T(8,128)(2,1)} fusion(bf16[1,384,2048]{2,1,0:T(8,128)(2,1)S(1)} %copy-done, bf16[1,2048,384]{2,1,0:T(8,128)(2,1)S(1)} %copy-done.10, bf16[8,1,64,2048]{3,2,1,0:T(8,128)(2,1)} %copy-done.1, f32[8,1,64,384]{3,2,0,1:T(8,128)} %fusion.30), kind=kOutput, calls=%fused_computation.32 | convolution fusion | flops 1612840960 | bytes 8126464 | tf_op jit(solution)/shard_map/sepf,efd->sepd/dot_general | solution.py:174
  178.3 4.5 %all-to-all-start.1 = ((bf16[8,1,64,2048]{3,2,1,0:T(8,128)(2,1)}), bf16[8,1,64,2048]{3,2,1,0:T(8,128)(2,1)}, u32[]{:S(2)}, u32[]{:S(2)}) async-start(bf16[8,1,64,2048]{3,2,1,0:T(8,128)(2,1)} %fusion.20), calls=%async_computation.2 | async-start | bytes 4194304 | tf_op jit(solution)/shard_map/all_to_all | solution.py:177
  182.8 0.4 fusion.88
  183.2 46.9 %all-to-all-done.1 = bf16[8,1,64,2048]{3,2,1,0:T(8,128)(2,1)} async-done(((bf16[8,1,64,2048]{3,2,1,0:T(8,128)(2,1)}), bf16[8,1,64,2048]{3,2,1,0:T(8,128)(2,1)}, u32[]{:S(2)}, u32[]{:S(2)}) %all-to-all-start.1) | async-done | bytes 2097184 | tf_op jit(solution)/shard_map/all_to_all | solution.py:177
  230.1 3.3 %fusion.29 = f32[64,2048]{1,0:T(8,128)} fusion(bf16[512,2048,1]{1,0,2:T(8,128)(2,1)} %bitcast.63, f32[64,4]{0,1:T(4,128)S(1)} %copy-done.11, s32[64,4]{0,1:T(4,128)S(1)} %multiply_add_fusion), kind=kOutput, calls=%fused_computation.43 | convolution fusion | flops 537919488 | bytes 2623488 | tf_op jit(solution)/shard_map/dot_general | solution.py:182
  233.4 3.1 %fusion.21 = bf16[64,2048]{1,0:T(8,128)(2,1)} fusion(bf16[384,2048]{1,0:T(8,128)(2,1)S(1)} %copy-done.2, bf16[2048,384]{1,0:T(8,128)(2,1)} %param.30, f32[64,2048]{1,0:T(8,128)} %fusion.29, bf16[64,2048]{1,0:T(8,128)(2,1)S(1)} %add_convert_fusion, f32[64,384]{1,0:T(8,128)S(1)} %fusion.88, f32[2048]{0:T(1024)S(1)} %copy-done.6, f32[64]{0:T(128)S(1)} %add_rsqrt_fusion), kind=kOutput, calls=%fused_computation.35 | convolution fusion | flops 202522624 | bytes 4301056 | tf_op jit(solution)/shard_map/dot_general | solution.py:190
  (53 shorter events, 0.3 us)
Async XLA Ops:
  6.5 166.3 %copy-start = (bf16[1,384,2048]{2,1,0:T(8,128)(2,1)S(1)}, bf16[1,384,2048]{2,1,0:T(8,128)(2,1)}, u32[]{:S(2)}) copy-start(bf16[1,384,2048]{2,1,0:T(8,128)(2,1)} %param.28) | copy-start | bytes 4718596
  6.5 107.2 %reduce-scatter.2.cloned.1.call-start = ((), (), s32[]{:S(2)}) async-start(), calls=%async_computation.3 | async-start | bytes 2621440 | tf_op jit(solution)/shard_map/reduce_scatter | solution.py:140
  9.2 1.1 copy-start.4
  9.7 0.9 copy-start.7
  10.7 7.6 %collective-permute-start = (bf16[2,256,128]{2,1,0:T(8,128)(2,1)S(1)}, bf16[2,256,128]{2,1,0:T(8,128)(2,1)S(1)}, u32[]{:S(2)}, u32[]{:S(2)}) collective-permute-start(bf16[2,256,128]{2,1,0:T(8,128)(2,1)S(1)} %get-tuple-element.332), channel_id=1, source_target_pairs={{0,4},{4,8},{8,12},{12,16},{16,20},{20,24},{24,28},{1,5},{5,9},{9,... | collective-permute-start | bytes 393224 | tf_op jit(solution)/shard_map/while/body/eval_jaxpr/ppermute | solution.py:17
  18.3 8.8 %collective-permute-start = (bf16[2,256,128]{2,1,0:T(8,128)(2,1)S(1)}, bf16[2,256,128]{2,1,0:T(8,128)(2,1)S(1)}, u32[]{:S(2)}, u32[]{:S(2)}) collective-permute-start(bf16[2,256,128]{2,1,0:T(8,128)(2,1)S(1)} %get-tuple-element.332), channel_id=1, source_target_pairs={{0,4},{4,8},{8,12},{12,16},{16,20},{20,24},{24,28},{1,5},{5,9},{9,... | collective-permute-start | bytes 393224 | tf_op jit(solution)/shard_map/while/body/eval_jaxpr/ppermute | solution.py:17
  27.2 6.9 %collective-permute-start = (bf16[2,256,128]{2,1,0:T(8,128)(2,1)S(1)}, bf16[2,256,128]{2,1,0:T(8,128)(2,1)S(1)}, u32[]{:S(2)}, u32[]{:S(2)}) collective-permute-start(bf16[2,256,128]{2,1,0:T(8,128)(2,1)S(1)} %get-tuple-element.332), channel_id=1, source_target_pairs={{0,4},{4,8},{8,12},{12,16},{16,20},{20,24},{24,28},{1,5},{5,9},{9,... | collective-permute-start | bytes 393224 | tf_op jit(solution)/shard_map/while/body/eval_jaxpr/ppermute | solution.py:17
  34.1 9.7 %collective-permute-start = (bf16[2,256,128]{2,1,0:T(8,128)(2,1)S(1)}, bf16[2,256,128]{2,1,0:T(8,128)(2,1)S(1)}, u32[]{:S(2)}, u32[]{:S(2)}) collective-permute-start(bf16[2,256,128]{2,1,0:T(8,128)(2,1)S(1)} %get-tuple-element.332), channel_id=1, source_target_pairs={{0,4},{4,8},{8,12},{12,16},{16,20},{20,24},{24,28},{1,5},{5,9},{9,... | collective-permute-start | bytes 393224 | tf_op jit(solution)/shard_map/while/body/eval_jaxpr/ppermute | solution.py:17
  43.8 7.8 %collective-permute-start = (bf16[2,256,128]{2,1,0:T(8,128)(2,1)S(1)}, bf16[2,256,128]{2,1,0:T(8,128)(2,1)S(1)}, u32[]{:S(2)}, u32[]{:S(2)}) collective-permute-start(bf16[2,256,128]{2,1,0:T(8,128)(2,1)S(1)} %get-tuple-element.332), channel_id=1, source_target_pairs={{0,4},{4,8},{8,12},{12,16},{16,20},{20,24},{24,28},{1,5},{5,9},{9,... | collective-permute-start | bytes 393224 | tf_op jit(solution)/shard_map/while/body/eval_jaxpr/ppermute | solution.py:17
  51.6 8.9 %collective-permute-start = (bf16[2,256,128]{2,1,0:T(8,128)(2,1)S(1)}, bf16[2,256,128]{2,1,0:T(8,128)(2,1)S(1)}, u32[]{:S(2)}, u32[]{:S(2)}) collective-permute-start(bf16[2,256,128]{2,1,0:T(8,128)(2,1)S(1)} %get-tuple-element.332), channel_id=1, source_target_pairs={{0,4},{4,8},{8,12},{12,16},{16,20},{20,24},{24,28},{1,5},{5,9},{9,... | collective-permute-start | bytes 393224 | tf_op jit(solution)/shard_map/while/body/eval_jaxpr/ppermute | solution.py:17
  60.5 7.5 %collective-permute-start = (bf16[2,256,128]{2,1,0:T(8,128)(2,1)S(1)}, bf16[2,256,128]{2,1,0:T(8,128)(2,1)S(1)}, u32[]{:S(2)}, u32[]{:S(2)}) collective-permute-start(bf16[2,256,128]{2,1,0:T(8,128)(2,1)S(1)} %get-tuple-element.332), channel_id=1, source_target_pairs={{0,4},{4,8},{8,12},{12,16},{16,20},{20,24},{24,28},{1,5},{5,9},{9,... | collective-permute-start | bytes 393224 | tf_op jit(solution)/shard_map/while/body/eval_jaxpr/ppermute | solution.py:17
  71.2 0.7 copy-start.8
  71.2 42.5 %copy-start.5 = (bf16[64,2048]{1,0:T(8,128)(2,1)S(1)}, bf16[64,2048]{1,0:T(8,128)(2,1)}, u32[]{:S(2)}) copy-start(bf16[64,2048]{1,0:T(8,128)(2,1)} %param.21) | copy-start | bytes 786436
  71.2 43.8 %copy-start.6 = (f32[2048]{0:T(1024)S(1)}, f32[2048]{0:T(1024)}, u32[]{:S(2)}) copy-start(f32[2048]{0:T(1024)} %param.23) | copy-start | bytes 24580
  115.8 54.8 %copy-start.9 = (bf16[1,2048,384]{2,1,0:T(8,128)(2,1)S(1)}, bf16[1,2048,384]{2,1,0:T(8,128)(2,1)}, u32[]{:S(2)}) copy-start(bf16[1,2048,384]{2,1,0:T(8,128)(2,1)} %param.26) | copy-start | bytes 4718596
  169.4 1.3 copy-start.1
  170.7 2.2 copy-start.10
  178.3 4.5 %copy-start.3 = (bf16[2048,384]{1,0:T(8,128)(2,1)S(1)}, bf16[2048,384]{1,0:T(8,128)(2,1)}, u32[]{:S(2)}) copy-start(bf16[2048,384]{1,0:T(8,128)(2,1)} %param.29) | copy-start | bytes 4718596
  178.3 51.8 %all-to-all-start.1 = ((bf16[8,1,64,2048]{3,2,1,0:T(8,128)(2,1)}), bf16[8,1,64,2048]{3,2,1,0:T(8,128)(2,1)}, u32[]{:S(2)}, u32[]{:S(2)}) async-start(bf16[8,1,64,2048]{3,2,1,0:T(8,128)(2,1)} %fusion.20), calls=%async_computation.2 | async-start | bytes 4194304 | tf_op jit(solution)/shard_map/all_to_all | solution.py:177
  182.8 47.3 %copy-start.11 = (f32[64,4]{0,1:T(4,128)S(1)}, f32[64,4]{0,1:T(4,128)}, u32[]{:S(2)}) copy-start(f32[64,4]{0,1:T(4,128)} %param.25) | copy-start | bytes 3076
  230.1 3.3 %copy-start.2 = (bf16[384,2048]{1,0:T(8,128)(2,1)S(1)}, bf16[384,2048]{1,0:T(8,128)(2,1)}, u32[]{:S(2)}) copy-start(bf16[384,2048]{1,0:T(8,128)(2,1)} %param.31) | copy-start | bytes 4718596
Sparse Core Ops, SparseCore 0:
  71.4 42.3 reduce-scatter.1
where the time goes:
time: 244 us; the launch traced here: 243 us
  waiting for transfers between devices  106 us (43%)
  blocking collectives  53.5 us (22%)
  starting transfers between devices  42.9 us (18%)
  matrix products  20.5 us (8%)
  between operations  13.6 us (6%)
  local copies, waits for them, and re-layouts  4.1 us (2%)
  other arithmetic  2.68 us (1%)
    all_to_all x1, blocking collectives, per_device(): lax.all_to_all(outgoing, 'sp', split_axis=0, concat_axis=0, tiled=True)  53.5 us
    all_to_all x1, waiting for transfers between devices, per_device(): lax.all_to_all(produced, 'sp', split_axis=0, concat_axis=0, tiled=True)  46.9 us
    reduce_scatter x1, waiting for transfers between devices, per_device(): lax.psum_scatter(jnp.dot(heads_out, out_weight, preferred_element_type=jn...  40.2 us
    ppermute x7, starting transfers between devices, shifted(): lax.ppermute(value, axis, [(source, source + steps) for source in range(f...  38.4 us
    ppermute x7, waiting for transfers between devices, shifted(): lax.ppermute(value, axis, [(source, source + steps) for source in range(f...  18.6 us
    dot_general x1, matrix products, per_device(): jnp.einsum('sepf,efd->sepd', hidden, expert_down, preferred_element_type=...  5.47 us
  transfers between devices with their start and end apart: 9, of which 9 were waited for; matrix products, arithmetic and copies ran while one was open for 1% of the time, Pallas kernels for 0%

commit v1 on v0

--- a/solution.py
+++ b/solution.py
@@ -1,8 +1,11 @@
+import functools
 import math
 
 import jax
 import jax.numpy as jnp
 from jax import lax
+from jax.experimental import pallas as pl
+from jax.experimental.pallas import tpu as pltpu
 from jax.sharding import PartitionSpec as P
 
 D = 2048
@@ -66,6 +69,241 @@
     values_split = shard_values.reshape(shard_values.shape[0], running.shape[0], running.shape[3])
     return running + jnp.einsum(
         "kgts,skd->kgtd", weights, values_split, preferred_element_type=jnp.float32
+    )
+
+
+MESH = pl.DeviceIdType.MESH
+
+
+def experts_kernel(
+    count,
+    x_ref,
+    mid_ref,
+    gate_hbm,
+    up_hbm,
+    down_hbm,
+    sgate_hbm,
+    sup_hbm,
+    sdown_hbm,
+    out_ref,
+    gate,
+    up,
+    down,
+    sgate,
+    sup,
+    sdown,
+    gathered,
+    kept,
+    pair_out,
+    pair_in,
+    line_out,
+    line_in,
+    load_sem,
+    xz_send,
+    xz_recv,
+    xy_send,
+    xy_recv,
+    py_send,
+    py_recv,
+    lz_send,
+    lz_recv,
+):
+    me = lax.axis_index("sp")
+    half = count // 2
+    rows, width = mid_ref.shape
+    place, side = me // 2, me % 2
+    partner = me + 1 - 2 * side
+
+    def along(distance):
+        return ((place + distance) % half) * 2 + side
+
+    loads = []
+    for number, (source, target) in enumerate(
+        (
+            (sgate_hbm, sgate),
+            (sup_hbm, sup),
+            (sdown_hbm, sdown),
+            (gate_hbm.at[0], gate),
+            (up_hbm.at[0], up),
+            (down_hbm.at[0], down),
+        )
+    ):
+        load = pltpu.make_async_copy(source, target, load_sem.at[number])
+        load.start()
+        loads.append(load)
+
+    barrier = pltpu.get_barrier_semaphore()
+    pl.semaphore_signal(barrier, inc=1, device_id={"sp": partner}, device_id_type=MESH)
+    for distance in range(1, half):
+        pl.semaphore_signal(
+            barrier, inc=1, device_id={"sp": along(distance)}, device_id_type=MESH
+        )
+    pl.semaphore_wait(barrier, half)
+
+    def remote(source, target, send, recv, device):
+        return pltpu.make_async_remote_copy(
+            src_ref=source,
+            dst_ref=target,
+            send_sem=send,
+            recv_sem=recv,
+            device_id={"sp": device},
+            device_id_type=MESH,
+        )
+
+    order = [0]
+    low, high = 1, half - 1
+    while low <= high:
+        order.append(low)
+        if high != low:
+            order.append(high)
+        low, high = low + 1, high - 1
+
+    top, bottom = pl.ds(0, rows), pl.ds(rows, rows)
+    across = {
+        d: remote(
+            x_ref if d == 0 else gathered.at[d, top],
+            gathered.at[d, bottom],
+            xy_send.at[d],
+            xy_recv.at[d],
+            partner,
+        )
+        for d in order
+    }
+    spread = {
+        d: remote(x_ref, gathered.at[d, top], xz_send.at[d], xz_recv.at[d], along(d))
+        for d in order[1:]
+    }
+    back = {
+        d: remote(pair_out.at[d], pair_in.at[d], py_send.at[d], py_recv.at[d], partner)
+        for d in order
+    }
+    home = {
+        d: remote(line_out.at[d], line_in.at[d], lz_send.at[d], lz_recv.at[d], along(half - d))
+        for d in order[1:]
+    }
+    across[0].start()
+    for d in order[1:]:
+        spread[d].start()
+    gathered[0, 0:rows] = x_ref[...]
+
+    def hidden_of(values, first, second):
+        a = jnp.dot(values, first[...], preferred_element_type=jnp.float32)
+        b = jnp.dot(values, second[...], preferred_element_type=jnp.float32)
+        return (a / (1.0 + jnp.exp(-a)) * b).astype(jnp.bfloat16)
+
+    for load in loads[:3]:
+        load.wait()
+    shared = hidden_of(x_ref[:, 0:width], sgate, sup)
+    kept[half] = mid_ref[...].astype(jnp.float32) + jnp.dot(
+        shared, sdown[...], preferred_element_type=jnp.float32
+    )
+    for load in loads[3:]:
+        load.wait()
+
+    def evaluate(d):
+        values = gathered[d]
+        extra = values[:, width:].astype(jnp.float32)
+        lane = lax.broadcasted_iota(jnp.int32, extra.shape, 1)
+        mine = (lane == me) | (lane == me + count)
+        weight = jnp.sum(jnp.where(mine, extra, 0.0), axis=1, keepdims=True)
+        hidden = hidden_of(values[:, 0:width], gate, up)
+        produced = jnp.dot(hidden, down[...], preferred_element_type=jnp.float32)
+        produced = produced.astype(jnp.bfloat16).astype(jnp.float32) * weight
+        pair_out[d] = produced[rows:].astype(jnp.bfloat16)
+        back[d].start()
+        kept[d] = produced[:rows]
+
+    def combine(d):
+        back[d].wait_recv()
+        total = kept[d] + pair_in[d].astype(jnp.float32)
+        if d == 0:
+            kept[half] = kept[half] + total
+        else:
+            line_out[d] = total.astype(jnp.bfloat16)
+            home[d].start()
+
+    for number in range(half + 1):
+        if number + 1 < half:
+            following = order[number + 1]
+            spread[following].wait_recv()
+            across[following].start()
+        if number < half:
+            across[order[number]].wait_recv()
+            evaluate(order[number])
+        if number >= 1:
+            combine(order[number - 1])
+
+    result = kept[half]
+    for d in order[1:]:
+        home[d].wait_recv()
+        result = result + line_in[d].astype(jnp.float32)
+    out_ref[...] = result.astype(out_ref.dtype)
+    for d in order:
+        across[d].wait_send()
+        back[d].wait_send()
+        if d != 0:
+            spread[d].wait_send()
+            home[d].wait_send()
+
+
+def dense_experts(
+    normed,
+    mid,
+    route_ids,
+    route_weights,
+    expert_gate,
+    expert_up,
+    expert_down,
+    shared_gate,
+    shared_up,
+    shared_down,
+):
+    count = lax.axis_size("sp")
+    half = count // 2
+    rows, width = normed.shape
+    extra = 128 * -(-2 * count // 128)
+    named = route_ids[:, :, None] == jnp.arange(count, dtype=jnp.int32)[None, None, :]
+    gates = jnp.sum(jnp.where(named, route_weights[:, :, None], 0.0), axis=1)
+    coarse = lax.reduce_precision(gates, 8, 7)
+    pieces = jnp.concatenate((coarse, gates - coarse), axis=1).astype(jnp.bfloat16)
+    pieces = jnp.pad(pieces, ((0, 0), (0, extra - 2 * count)))
+    extended = jnp.concatenate((normed, pieces), axis=1)
+    fe, sh = expert_gate.shape[2], shared_gate.shape[1]
+    vmem, anywhere = pl.BlockSpec(memory_space=pltpu.VMEM), pl.BlockSpec(memory_space=pl.ANY)
+    bf16 = jnp.bfloat16
+    return pl.pallas_call(
+        functools.partial(experts_kernel, count),
+        out_shape=jax.ShapeDtypeStruct((rows, width), jnp.bfloat16),
+        in_specs=[vmem] * 2 + [anywhere] * 6,
+        out_specs=vmem,
+        scratch_shapes=[
+            pltpu.VMEM((width, fe), bf16),
+            pltpu.VMEM((width, fe), bf16),
+            pltpu.VMEM((fe, width), bf16),
+            pltpu.VMEM((width, sh), bf16),
+            pltpu.VMEM((width, sh), bf16),
+            pltpu.VMEM((sh, width), bf16),
+            pltpu.VMEM((half, 2 * rows, width + extra), bf16),
+            pltpu.VMEM((half + 1, rows, width), jnp.float32),
+            pltpu.VMEM((half, rows, width), bf16),
+            pltpu.VMEM((half, rows, width), bf16),
+            pltpu.VMEM((half, rows, width), bf16),
+            pltpu.VMEM((half, rows, width), bf16),
+            pltpu.SemaphoreType.DMA((6,)),
+        ]
+        + [pltpu.SemaphoreType.DMA((half,))] * 8,
+        compiler_params=pltpu.CompilerParams(
+            collective_id=1, has_side_effects=True, vmem_limit_bytes=48 * 1024 * 1024
+        ),
+    )(
+        extended,
+        mid,
+        expert_gate,
+        expert_up,
+        expert_down,
+        shared_gate,
+        shared_up,
+        shared_down,
     )
 
 
@@ -153,6 +391,19 @@
     local_experts = expert_gate.shape[0]
     expert_count = lax.axis_size("sp") * local_experts
     capacity = 2 * own_rows * TOP_K // expert_count
+    if capacity >= own_rows and local_experts == 1 and expert_count % 2 == 0:
+        return dense_experts(
+            normed,
+            mid,
+            route_ids,
+            route_weights,
+            expert_gate,
+            expert_up,
+            expert_down,
+            shared_gate,
+            shared_up,
+            shared_down,
+        )
     slot_count = expert_count * capacity
     flat_ids = route_ids.reshape(-1)
     membership = (flat_ids[:, None] == jnp.arange(expert_count, dtype=jnp.int32)[None, :]).astype(

time: 244 us -> 189 us (0.77)
  Pallas kernels: 0 us -> 63.8 us
  blocking collectives: 53.5 us -> 0 us
  waiting for transfers between devices: 106 us -> 60.4 us
  matrix products: 20.5 us -> 4.04 us
  starting transfers between devices: 42.9 us -> 38.4 us
    pallas_call x0 -> x1, Pallas kernels: none -> 63.8 us  [dense_experts(): pl.pallas_call(functools.partial(experts_kernel, count), out_shape=jax.Sh...]
    all_to_all x1 -> x0, blocking collectives: 53.5 us -> none  [per_device(): lax.all_to_all(outgoing, 'sp', split_axis=0, concat_axis=0, tiled=True)]
    all_to_all x1 -> x0, waiting for transfers between devices: 46.9 us -> none  [per_device(): lax.all_to_all(produced, 'sp', split_axis=0, concat_axis=0, tiled=True)]
    dot_general x6 -> x0, matrix products: 15.2 us -> none  [the longest x1 5.47 us: per_device(): jnp.einsum('sepf,efd->sepd', hidden, expert_down, preferred_element_type=...]
    all_to_all x1 -> x0, starting transfers between devices: 4.5 us -> none  [per_device(): lax.all_to_all(produced, 'sp', split_axis=0, concat_axis=0, tiled=True)]
    unnamed x27 -> x23, local copies, waits for them, and re-layouts: 3.31 us -> 5.4 us
  transfers between devices with their start and end apart: 9 -> 8, of which waited for: 9 -> 8; matrix products, arithmetic and copies ran while one was open for 1% -> 0% of each run, Pallas kernels for 0% -> 0%
where the time goes in v1:
time: 189 us; the launch traced here: 188 us
  Pallas kernels  63.8 us (34%)
  waiting for transfers between devices  60.4 us (32%)
  starting transfers between devices  38.4 us (20%)
  between operations  13.6 us (7%)
  local copies, waits for them, and re-layouts  5.68 us (3%)
  matrix products  4.04 us (2%)
  other arithmetic  1.99 us (1%)
    pallas_call x1, Pallas kernels, dense_experts(): pl.pallas_call(functools.partial(experts_kernel, count), out_shape=jax.Sh...  63.8 us
    reduce_scatter x1, waiting for transfers between devices, per_device(): lax.psum_scatter(jnp.dot(heads_out, out_weight, preferred_element_type=jn...  41.7 us
    ppermute x7, starting transfers between devices, shifted(): lax.ppermute(value, axis, [(source, source + steps) for source in range(f...  38.4 us
    ppermute x7, waiting for transfers between devices, shifted(): lax.ppermute(value, axis, [(source, source + steps) for source in range(f...  18.7 us
    unnamed x23, local copies, waits for them, and re-layouts  5.4 us
  transfers between devices with their start and end apart: 8, of which 8 were waited for; matrix products, arithmetic and copies ran while one was open for 0% of the time, Pallas kernels for 0%

profile of v1, /device:TPU:0, one launch (start us, length us, event | category | flops | bytes accessed | tf_op | source)
XLA Modules:
  0.0 188.1 jit_solution(17079864683530371887)
XLA Ops:
  6.5 0.0 copy-start
  6.5 0.0 reduce-scatter.2.cloned.1.call-start
  6.5 0.1 broadcast_compare_fusion.1
  6.7 1.1 copy.48
  7.7 1.5 fusion.44
  9.2 0.0 copy-start.4
  9.2 0.4 fusion.35
  9.6 0.0 copy-start.6
  9.7 0.1 fusion.38
  9.8 0.1 copy.49
  9.9 0.4 fusion.27
  10.3 0.0 copy-done.4
  10.3 0.3 convolution_bitcast_fusion.1
  10.6 0.0 copy-done.6
  10.6 57.4 %while.19 = (s32[]{:T(128)}, f32[1,2,256,128]{3,2,1,0:T(8,128)S(1)}, f32[1,2,256]{2,1,0:T(2,128)S(1)}, bf16[2,256,128]{2,1,0:T(8,128)(2,1)S(1)}, s32[]{:T(128)},...) while((s32[]{:T(128)}, f32[1,2,256,128]{3,2,1,0:T(8,128)S(1)}, ...), condition=%wide.region_7.8_spmd.clone.clone, body=%wide.region_2.7_spmd.clone.clone.sunk | while | flops 270967296 | bytes 5996823 | solution.py:371
  10.6 4.9 %collective-permute-start = (bf16[2,256,128]{2,1,0:T(8,128)(2,1)S(1)}, bf16[2,256,128]{2,1,0:T(8,128)(2,1)S(1)}, u32[]{:S(2)}, u32[]{:S(2)}) collective-permute-start(bf16[2,256,128]{2,1,0:T(8,128)(2,1)S(1)} %get-tuple-element.327), channel_id=1, source_target_pairs={{0,4},{4,8},{8,12},{12,16},{16,20},{20,24},{24,28},{1,5},{5,9},{9,... | collective-permute-start | bytes 393224 | tf_op jit(solution)/shard_map/while/body/eval_jaxpr/ppermute | solution.py:20
  15.6 2.7 %collective-permute-done = bf16[2,256,128]{2,1,0:T(8,128)(2,1)S(1)} collective-permute-done((bf16[2,256,128]{2,1,0:T(8,128)(2,1)S(1)}, bf16[2,256,128]{2,1,0:T(8,128)(2,1)S(1)}, u32[]{:S(2)}, u32[]{:S(2)}) %collective-permute-start) | collective-permute-done | bytes 131104 | tf_op jit(solution)/shard_map/while/body/eval_jaxpr/ppermute | solution.py:20
  18.3 6.3 %collective-permute-start = (bf16[2,256,128]{2,1,0:T(8,128)(2,1)S(1)}, bf16[2,256,128]{2,1,0:T(8,128)(2,1)S(1)}, u32[]{:S(2)}, u32[]{:S(2)}) collective-permute-start(bf16[2,256,128]{2,1,0:T(8,128)(2,1)S(1)} %get-tuple-element.327), channel_id=1, source_target_pairs={{0,4},{4,8},{8,12},{12,16},{16,20},{20,24},{24,28},{1,5},{5,9},{9,... | collective-permute-start | bytes 393224 | tf_op jit(solution)/shard_map/while/body/eval_jaxpr/ppermute | solution.py:20
  24.6 2.5 %collective-permute-done = bf16[2,256,128]{2,1,0:T(8,128)(2,1)S(1)} collective-permute-done((bf16[2,256,128]{2,1,0:T(8,128)(2,1)S(1)}, bf16[2,256,128]{2,1,0:T(8,128)(2,1)S(1)}, u32[]{:S(2)}, u32[]{:S(2)}) %collective-permute-start) | collective-permute-done | bytes 131104 | tf_op jit(solution)/shard_map/while/body/eval_jaxpr/ppermute | solution.py:20
  27.2 4.4 %collective-permute-start = (bf16[2,256,128]{2,1,0:T(8,128)(2,1)S(1)}, bf16[2,256,128]{2,1,0:T(8,128)(2,1)S(1)}, u32[]{:S(2)}, u32[]{:S(2)}) collective-permute-start(bf16[2,256,128]{2,1,0:T(8,128)(2,1)S(1)} %get-tuple-element.327), channel_id=1, source_target_pairs={{0,4},{4,8},{8,12},{12,16},{16,20},{20,24},{24,28},{1,5},{5,9},{9,... | collective-permute-start | bytes 393224 | tf_op jit(solution)/shard_map/while/body/eval_jaxpr/ppermute | solution.py:20
  31.5 2.5 %collective-permute-done = bf16[2,256,128]{2,1,0:T(8,128)(2,1)S(1)} collective-permute-done((bf16[2,256,128]{2,1,0:T(8,128)(2,1)S(1)}, bf16[2,256,128]{2,1,0:T(8,128)(2,1)S(1)}, u32[]{:S(2)}, u32[]{:S(2)}) %collective-permute-start) | collective-permute-done | bytes 131104 | tf_op jit(solution)/shard_map/while/body/eval_jaxpr/ppermute | solution.py:20
  34.1 7.2 %collective-permute-start = (bf16[2,256,128]{2,1,0:T(8,128)(2,1)S(1)}, bf16[2,256,128]{2,1,0:T(8,128)(2,1)S(1)}, u32[]{:S(2)}, u32[]{:S(2)}) collective-permute-start(bf16[2,256,128]{2,1,0:T(8,128)(2,1)S(1)} %get-tuple-element.327), channel_id=1, source_target_pairs={{0,4},{4,8},{8,12},{12,16},{16,20},{20,24},{24,28},{1,5},{5,9},{9,... | collective-permute-start | bytes 393224 | tf_op jit(solution)/shard_map/while/body/eval_jaxpr/ppermute | solution.py:20
  41.2 2.5 %collective-permute-done = bf16[2,256,128]{2,1,0:T(8,128)(2,1)S(1)} collective-permute-done((bf16[2,256,128]{2,1,0:T(8,128)(2,1)S(1)}, bf16[2,256,128]{2,1,0:T(8,128)(2,1)S(1)}, u32[]{:S(2)}, u32[]{:S(2)}) %collective-permute-start) | collective-permute-done | bytes 131104 | tf_op jit(solution)/shard_map/while/body/eval_jaxpr/ppermute | solution.py:20
  43.8 5.3 %collective-permute-start = (bf16[2,256,128]{2,1,0:T(8,128)(2,1)S(1)}, bf16[2,256,128]{2,1,0:T(8,128)(2,1)S(1)}, u32[]{:S(2)}, u32[]{:S(2)}) collective-permute-start(bf16[2,256,128]{2,1,0:T(8,128)(2,1)S(1)} %get-tuple-element.327), channel_id=1, source_target_pairs={{0,4},{4,8},{8,12},{12,16},{16,20},{20,24},{24,28},{1,5},{5,9},{9,... | collective-permute-start | bytes 393224 | tf_op jit(solution)/shard_map/while/body/eval_jaxpr/ppermute | solution.py:20
  49.0 2.5 %collective-permute-done = bf16[2,256,128]{2,1,0:T(8,128)(2,1)S(1)} collective-permute-done((bf16[2,256,128]{2,1,0:T(8,128)(2,1)S(1)}, bf16[2,256,128]{2,1,0:T(8,128)(2,1)S(1)}, u32[]{:S(2)}, u32[]{:S(2)}) %collective-permute-start) | collective-permute-done | bytes 131104 | tf_op jit(solution)/shard_map/while/body/eval_jaxpr/ppermute | solution.py:20
  51.5 5.4 %collective-permute-start = (bf16[2,256,128]{2,1,0:T(8,128)(2,1)S(1)}, bf16[2,256,128]{2,1,0:T(8,128)(2,1)S(1)}, u32[]{:S(2)}, u32[]{:S(2)}) collective-permute-start(bf16[2,256,128]{2,1,0:T(8,128)(2,1)S(1)} %get-tuple-element.327), channel_id=1, source_target_pairs={{0,4},{4,8},{8,12},{12,16},{16,20},{20,24},{24,28},{1,5},{5,9},{9,... | collective-permute-start | bytes 393224 | tf_op jit(solution)/shard_map/while/body/eval_jaxpr/ppermute | solution.py:20
  57.0 3.5 %collective-permute-done = bf16[2,256,128]{2,1,0:T(8,128)(2,1)S(1)} collective-permute-done((bf16[2,256,128]{2,1,0:T(8,128)(2,1)S(1)}, bf16[2,256,128]{2,1,0:T(8,128)(2,1)S(1)}, u32[]{:S(2)}, u32[]{:S(2)}) %collective-permute-start) | collective-permute-done | bytes 131104 | tf_op jit(solution)/shard_map/while/body/eval_jaxpr/ppermute | solution.py:20
  60.5 5.0 %collective-permute-start = (bf16[2,256,128]{2,1,0:T(8,128)(2,1)S(1)}, bf16[2,256,128]{2,1,0:T(8,128)(2,1)S(1)}, u32[]{:S(2)}, u32[]{:S(2)}) collective-permute-start(bf16[2,256,128]{2,1,0:T(8,128)(2,1)S(1)} %get-tuple-element.327), channel_id=1, source_target_pairs={{0,4},{4,8},{8,12},{12,16},{16,20},{20,24},{24,28},{1,5},{5,9},{9,... | collective-permute-start | bytes 393224 | tf_op jit(solution)/shard_map/while/body/eval_jaxpr/ppermute | solution.py:20
  65.5 2.5 %collective-permute-done = bf16[2,256,128]{2,1,0:T(8,128)(2,1)S(1)} collective-permute-done((bf16[2,256,128]{2,1,0:T(8,128)(2,1)S(1)}, bf16[2,256,128]{2,1,0:T(8,128)(2,1)S(1)}, u32[]{:S(2)}, u32[]{:S(2)}) %collective-permute-start) | collective-permute-done | bytes 131104 | tf_op jit(solution)/shard_map/while/body/eval_jaxpr/ppermute | solution.py:20
  68.1 0.1 copy.50
  68.2 0.0 copy-done
  68.2 1.8 fusion.45
  70.0 0.0 reduce-scatter.2.cloned.1.call-update
  70.0 0.6 copy-done.8
  70.7 0.0 copy-done.9
  70.7 0.1 copy.51
  70.8 41.7 %reduce-scatter.2.cloned.1.call-done = f32[64,2048]{1,0:T(8,128)} async-done(((f32[256,2048]{1,0:T(8,128)}), f32[64,2048]{1,0:T(8,128)}) %reduce-scatter.2.cloned.1.call-update) | async-done | bytes 524304 | tf_op jit(solution)/shard_map/reduce_scatter | solution.py:378
  112.6 0.0 copy-done.5
  112.6 1.1 add_convert_fusion.mid_ref
  113.6 0.2 fusion.22
  113.8 0.0 copy-done.7
  113.8 0.1 fusion.24
  114.0 0.0 copy-done.1
  114.0 0.0 copy-start.2
  114.0 1.4 copy-done.2
  115.4 1.4 copy-done.3
  116.8 63.8 %shard_map.136 = bf16[64,2048]{1,0:T(8,128)(2,1)S(1)} custom-call(bf16[64,2176]{1,0:T(8,128)(2,1)S(1)} %fusion.28.x_ref, bf16[64,2048]{1,0:T(8,128)(2,1)S(1)} %add_convert_fusion.mid_ref, bf16[1,2048,384]{2,1,0:T(8,128)(2,1)S(1)} %copy-done.1, bf16[1,2048,384]{2,1,0:T(8,128)(2,1)S(1)} %copy-done.2, bf16[1,384,2048]{2,1,0:T(8,128)(2,1)S(1)} %copy-done.3, ...), custom_call_target="tpu_custom_call" | custom-call | tf_op jit(solution)/shard_map/pallas_call | solution.py:274
  180.6 0.7 copy.84
  (35 shorter events, 0.2 us)
Async XLA Ops:
  6.5 61.6 %copy-start = (bf16[256,2048]{1,0:T(8,128)(2,1)S(1)}, bf16[256,2048]{1,0:T(8,128)(2,1)}, u32[]{:S(2)}) copy-start(bf16[256,2048]{1,0:T(8,128)(2,1)} %param.22) | copy-start | bytes 3145732
  6.5 106.0 %reduce-scatter.2.cloned.1.call-start = ((), (), s32[]{:S(2)}) async-start(), calls=%async_computation.1 | async-start | bytes 2621440 | tf_op jit(solution)/shard_map/reduce_scatter | solution.py:378
  9.2 1.1 copy-start.4
  9.6 1.0 copy-start.6
  10.6 7.6 %collective-permute-start = (bf16[2,256,128]{2,1,0:T(8,128)(2,1)S(1)}, bf16[2,256,128]{2,1,0:T(8,128)(2,1)S(1)}, u32[]{:S(2)}, u32[]{:S(2)}) collective-permute-start(bf16[2,256,128]{2,1,0:T(8,128)(2,1)S(1)} %get-tuple-element.327), channel_id=1, source_target_pairs={{0,4},{4,8},{8,12},{12,16},{16,20},{20,24},{24,28},{1,5},{5,9},{9,... | collective-permute-start | bytes 393224 | tf_op jit(solution)/shard_map/while/body/eval_jaxpr/ppermute | solution.py:20
  18.3 8.8 %collective-permute-start = (bf16[2,256,128]{2,1,0:T(8,128)(2,1)S(1)}, bf16[2,256,128]{2,1,0:T(8,128)(2,1)S(1)}, u32[]{:S(2)}, u32[]{:S(2)}) collective-permute-start(bf16[2,256,128]{2,1,0:T(8,128)(2,1)S(1)} %get-tuple-element.327), channel_id=1, source_target_pairs={{0,4},{4,8},{8,12},{12,16},{16,20},{20,24},{24,28},{1,5},{5,9},{9,... | collective-permute-start | bytes 393224 | tf_op jit(solution)/shard_map/while/body/eval_jaxpr/ppermute | solution.py:20
  27.2 6.9 %collective-permute-start = (bf16[2,256,128]{2,1,0:T(8,128)(2,1)S(1)}, bf16[2,256,128]{2,1,0:T(8,128)(2,1)S(1)}, u32[]{:S(2)}, u32[]{:S(2)}) collective-permute-start(bf16[2,256,128]{2,1,0:T(8,128)(2,1)S(1)} %get-tuple-element.327), channel_id=1, source_target_pairs={{0,4},{4,8},{8,12},{12,16},{16,20},{20,24},{24,28},{1,5},{5,9},{9,... | collective-permute-start | bytes 393224 | tf_op jit(solution)/shard_map/while/body/eval_jaxpr/ppermute | solution.py:20
  34.1 9.7 %collective-permute-start = (bf16[2,256,128]{2,1,0:T(8,128)(2,1)S(1)}, bf16[2,256,128]{2,1,0:T(8,128)(2,1)S(1)}, u32[]{:S(2)}, u32[]{:S(2)}) collective-permute-start(bf16[2,256,128]{2,1,0:T(8,128)(2,1)S(1)} %get-tuple-element.327), channel_id=1, source_target_pairs={{0,4},{4,8},{8,12},{12,16},{16,20},{20,24},{24,28},{1,5},{5,9},{9,... | collective-permute-start | bytes 393224 | tf_op jit(solution)/shard_map/while/body/eval_jaxpr/ppermute | solution.py:20
  43.8 7.8 %collective-permute-start = (bf16[2,256,128]{2,1,0:T(8,128)(2,1)S(1)}, bf16[2,256,128]{2,1,0:T(8,128)(2,1)S(1)}, u32[]{:S(2)}, u32[]{:S(2)}) collective-permute-start(bf16[2,256,128]{2,1,0:T(8,128)(2,1)S(1)} %get-tuple-element.327), channel_id=1, source_target_pairs={{0,4},{4,8},{8,12},{12,16},{16,20},{20,24},{24,28},{1,5},{5,9},{9,... | collective-permute-start | bytes 393224 | tf_op jit(solution)/shard_map/while/body/eval_jaxpr/ppermute | solution.py:20
  51.5 8.9 %collective-permute-start = (bf16[2,256,128]{2,1,0:T(8,128)(2,1)S(1)}, bf16[2,256,128]{2,1,0:T(8,128)(2,1)S(1)}, u32[]{:S(2)}, u32[]{:S(2)}) collective-permute-start(bf16[2,256,128]{2,1,0:T(8,128)(2,1)S(1)} %get-tuple-element.327), channel_id=1, source_target_pairs={{0,4},{4,8},{8,12},{12,16},{16,20},{20,24},{24,28},{1,5},{5,9},{9,... | collective-permute-start | bytes 393224 | tf_op jit(solution)/shard_map/while/body/eval_jaxpr/ppermute | solution.py:20
  60.5 7.5 %collective-permute-start = (bf16[2,256,128]{2,1,0:T(8,128)(2,1)S(1)}, bf16[2,256,128]{2,1,0:T(8,128)(2,1)S(1)}, u32[]{:S(2)}, u32[]{:S(2)}) collective-permute-start(bf16[2,256,128]{2,1,0:T(8,128)(2,1)S(1)} %get-tuple-element.327), channel_id=1, source_target_pairs={{0,4},{4,8},{8,12},{12,16},{16,20},{20,24},{24,28},{1,5},{5,9},{9,... | collective-permute-start | bytes 393224 | tf_op jit(solution)/shard_map/while/body/eval_jaxpr/ppermute | solution.py:20
  70.0 0.7 copy-start.8
  70.0 0.7 copy-start.9
  70.0 42.6 %copy-start.5 = (bf16[64,2048]{1,0:T(8,128)(2,1)S(1)}, bf16[64,2048]{1,0:T(8,128)(2,1)}, u32[]{:S(2)}) copy-start(bf16[64,2048]{1,0:T(8,128)(2,1)} %param.21) | copy-start | bytes 786436
  70.0 43.8 %copy-start.7 = (f32[2048]{0:T(1024)S(1)}, f32[2048]{0:T(1024)}, u32[]{:S(2)}) copy-start(f32[2048]{0:T(1024)} %param.23) | copy-start | bytes 24580
  70.7 43.3 %copy-start.1 = (bf16[1,2048,384]{2,1,0:T(8,128)(2,1)S(1)}, bf16[1,2048,384]{2,1,0:T(8,128)(2,1)}, u32[]{:S(2)}) copy-start(bf16[1,2048,384]{2,1,0:T(8,128)(2,1)} %gate_hbm.1) | copy-start | bytes 4718596
  114.0 1.4 copy-start.2
  115.4 1.4 copy-start.3
Sparse Core Ops, SparseCore 0:
  70.1 42.3 reduce-scatter.1

commit v2 on v1

--- a/solution.py
+++ b/solution.py
@@ -246,28 +246,304 @@
             home[d].wait_send()
 
 
-def dense_experts(
-    normed,
-    mid,
-    route_ids,
-    route_weights,
-    expert_gate,
-    expert_up,
-    expert_down,
-    shared_gate,
-    shared_up,
-    shared_down,
+def attention_kernel(
+    count,
+    peers,
+    q_ref,
+    kv_ref,
+    w_hbm,
+    stream_ref,
+    gain_ref,
+    pieces_ref,
+    ext_ref,
+    mid_ref,
+    shards,
+    weights,
+    later,
+    mixed,
+    carried,
+    leaving,
+    heads,
+    load_sem,
+    line_send,
+    line_recv,
+    pair_send,
+    pair_recv,
+    wx_send,
+    wx_recv,
+    wc_send,
+    wc_recv,
+    row_send,
+    row_recv,
 ):
+    me, lane_pos = lax.axis_index("sp"), lax.axis_index("tp")
+    half, chips = count // 2, peers // 2
+    place, side = me // 2, me % 2
+    partner = me + 1 - 2 * side
+    onward, previous = (me + 2) % count, (me + count - 2) % count
+    chip, core = lane_pos // 2, lane_pos % 2
+    core_mate = lane_pos + 1 - 2 * core
+    tokens, own_rows = q_ref.shape[0], stream_ref.shape[0]
+    groups = q_ref.shape[1] // HD
+    scale = math.log2(math.e) / math.sqrt(HD)
+
+    load = pltpu.make_async_copy(w_hbm, weights.at[lane_pos], load_sem)
+    load.start()
+    barrier = pltpu.get_barrier_semaphore()
+    for device in (partner, onward, previous):
+        pl.semaphore_signal(barrier, inc=1, device_id={"sp": device}, device_id_type=MESH)
+    for step in range(1, peers):
+        pl.semaphore_signal(
+            barrier, inc=1, device_id={"tp": (lane_pos + step) % peers}, device_id_type=MESH
+        )
+    pl.semaphore_wait(barrier, 3 + peers - 1)
+
+    def remote(source, target, send, recv, **device):
+        return pltpu.make_async_remote_copy(
+            src_ref=source,
+            dst_ref=target,
+            send_sem=send,
+            recv_sem=recv,
+            device_id=device,
+            device_id_type=MESH,
+        )
+
+    def held(d):
+        return kv_ref if d == 0 else shards.at[d, side]
+
+    line = {
+        d: remote(held(d - 1), shards.at[d, side], line_send.at[d], line_recv.at[d], sp=onward)
+        for d in range(1, half)
+    }
+    pair = {
+        d: remote(held(d), shards.at[d, side], pair_send.at[d], pair_recv.at[d], sp=partner)
+        for d in range(half)
+    }
+    chip_copy = {
+        step: remote(
+            weights.at[lane_pos],
+            weights.at[lane_pos],
+            wx_send.at[step],
+            wx_recv.at[step],
+            tp=((chip + step) % chips) * 2 + core,
+        )
+        for step in range(1, chips)
+    }
+
+    def core_copy(step):
+        source = ((chip + chips - step) % chips) * 2 + core
+        return remote(
+            weights.at[source],
+            weights.at[source],
+            wc_send.at[step],
+            wc_recv.at[step],
+            tp=core_mate,
+        )
+
+    @pl.when(place + 1 < half)
+    def _():
+        line[1].start()
+
+    @pl.when(side == 0)
+    def _():
+        pair[0].start()
+
+    load.wait()
+    for step in range(1, chips):
+        chip_copy[step].start()
+    core_copy(0).start()
+
+    row_pos = lax.broadcasted_iota(jnp.int32, (tokens, tokens), 0)
+    key_pos = lax.broadcasted_iota(jnp.int32, (tokens, tokens), 1)
+    later[...] = (row_pos > key_pos).astype(jnp.float32).astype(jnp.bfloat16)
+
+    def visit(keys, values, diagonal):
+        for group in range(groups):
+            queries = q_ref[:, group * HD : (group + 1) * HD]
+            logits = scale * lax.dot_general(
+                queries, keys, (((1,), (1,)), ((), ())), preferred_element_type=jnp.float32
+            )
+            tail = jnp.log2(1.0 + jnp.exp2(-jnp.abs(logits)))
+            penalty = jnp.maximum(logits, 0.0) + tail
+            start = jnp.minimum(logits, 0.0) - tail
+            if diagonal:
+                visible = key_pos < row_pos
+                penalty = jnp.where(visible, penalty, 0.0)
+            coarse = penalty.astype(jnp.bfloat16)
+            fine = (penalty - coarse.astype(jnp.float32)).astype(jnp.bfloat16)
+            inside = jnp.dot(coarse, later[...], preferred_element_type=jnp.float32) + jnp.dot(
+                fine, later[...], preferred_element_type=jnp.float32
+            )
+            total = inside[:, 0:1] + penalty[:, 0:1]
+            if diagonal:
+                stick = jnp.where(visible, jnp.exp2(start - inside), 0.0)
+            else:
+                stick = jnp.exp2(start - (inside + carried[group][:, 0:1]))
+            part = jnp.dot(
+                stick.astype(jnp.bfloat16), values, preferred_element_type=jnp.float32
+            )
+            if diagonal:
+                mixed[group] = part
+                carried[group] = jnp.broadcast_to(total, (tokens, HD))
+            else:
+                mixed[group] = mixed[group] + part
+                carried[group] = carried[group] + total
+
+    visit(kv_ref[:, 0:HD], kv_ref[:, HD : 2 * HD], True)
+
+    def relay(d):
+        @pl.when(place >= d)
+        def _():
+            line[d].wait_recv()
+            pair[d].start()
+
+        if d + 1 < half:
+
+            @pl.when((place >= d) & (place + 1 < half))
+            def _():
+                line[d + 1].start()
+
+    for d in range(half):
+        if d + 1 < half:
+            relay(d + 1)
+        if d == 0:
+
+            @pl.when(side == 1)
+            def _():
+                arrival = remote(
+                    kv_ref,
+                    shards.at[0, 1 - side],
+                    pair_send.at[0],
+                    pair_recv.at[0],
+                    sp=partner,
+                )
+                arrival.wait_recv()
+                visit(shards[0, 0, :, 0:HD], shards[0, 0, :, HD : 2 * HD], False)
+
+        else:
+
+            @pl.when(place >= d)
+            def _():
+                pair[d].wait_recv()
+                for which in (1, 0):
+                    visit(shards[d, which, :, 0:HD], shards[d, which, :, HD : 2 * HD], False)
+
+    for group in range(groups):
+        leaving[:, group * HD : (group + 1) * HD] = mixed[group].astype(jnp.bfloat16)
+    rows_to = {}
+    for step in range(1, peers):
+        target = (lane_pos + step) % peers
+        rows_to[step] = remote(
+            leaving.at[pl.ds(pl.multiple_of(target * own_rows, own_rows), own_rows)],
+            heads.at[step],
+            row_send.at[step],
+            row_recv.at[step],
+            tp=target,
+        )
+        rows_to[step].start()
+    own = leaving[pl.ds(pl.multiple_of(lane_pos * own_rows, own_rows), own_rows), :]
+    total = stream_ref[...].astype(jnp.float32) + jnp.dot(
+        own, weights[lane_pos], preferred_element_type=jnp.float32
+    )
+    for step in range(1, chips):
+        chip_copy[step].wait_recv()
+        core_copy(step).start()
+    for step in range(1, peers):
+        rows_to[step].wait_recv()
+    for step in range(chips):
+        core_copy(step).wait_recv()
+    for step in range(1, peers):
+        source = (lane_pos + peers - step) % peers
+        total = total + jnp.dot(heads[step], weights[source], preferred_element_type=jnp.float32)
+    mid = total.astype(jnp.bfloat16)
+    mid_ref[...] = mid
+    wide = mid.astype(jnp.float32)
+    power = jnp.mean(wide * wide, axis=1, keepdims=True)
+    width = mid.shape[1]
+    ext_ref[:, 0:width] = (wide * lax.rsqrt(power + 1e-06) * gain_ref[...]).astype(jnp.bfloat16)
+    ext_ref[:, width:] = pieces_ref[...]
+
+    @pl.when(side == 0)
+    def _():
+        pair[0].wait_send()
+
+    for d in range(1, half):
+
+        @pl.when(place >= d)
+        def _():
+            pair[d].wait_send()
+
+        @pl.when((place + 1 >= d) & (place + 1 < half))
+        def _():
+            line[d].wait_send()
+
+    for step in range(1, chips):
+        chip_copy[step].wait_send()
+    for step in range(chips):
+        core_copy(step).wait_send()
+    for step in range(1, peers):
+        rows_to[step].wait_send()
+
+
+def attend(query, key_rows, value_rows, out_weight, stream, norm_gain, pieces):
+    count, peers = lax.axis_size("sp"), lax.axis_size("tp")
+    half, chips = count // 2, peers // 2
+    tokens, own_rows, width = query.shape[0], stream.shape[0], stream.shape[1]
+    groups = query.shape[1] // HD
+    vmem, anywhere = pl.BlockSpec(memory_space=pltpu.VMEM), pl.BlockSpec(memory_space=pl.ANY)
+    bf16 = jnp.bfloat16
+    dma = pltpu.SemaphoreType.DMA
+    return pl.pallas_call(
+        functools.partial(attention_kernel, count, peers),
+        out_shape=(
+            jax.ShapeDtypeStruct((own_rows, width + pieces.shape[1]), bf16),
+            jax.ShapeDtypeStruct((own_rows, width), bf16),
+        ),
+        in_specs=[vmem, vmem, anywhere, vmem, vmem, vmem],
+        out_specs=(vmem, vmem),
+        scratch_shapes=[
+            pltpu.VMEM((half, 2, tokens, 2 * HD), bf16),
+            pltpu.VMEM((peers,) + out_weight.shape, bf16),
+            pltpu.VMEM((tokens, tokens), bf16),
+            pltpu.VMEM((groups, tokens, HD), jnp.float32),
+            pltpu.VMEM((groups, tokens, HD), jnp.float32),
+            pltpu.VMEM((tokens, groups * HD), bf16),
+            pltpu.VMEM((peers, own_rows, groups * HD), bf16),
+            dma,
+        ]
+        + [dma((half,))] * 4
+        + [dma((chips,))] * 4
+        + [dma((peers,))] * 2,
+        compiler_params=pltpu.CompilerParams(
+            collective_id=2, has_side_effects=True, vmem_limit_bytes=40 * 1024 * 1024
+        ),
+    )(
+        query,
+        jnp.concatenate((key_rows, value_rows), axis=1),
+        out_weight,
+        stream,
+        norm_gain.reshape(1, width),
+        pieces,
+    )
+
+
+def gate_pieces(route_ids, route_weights):
     count = lax.axis_size("sp")
-    half = count // 2
-    rows, width = normed.shape
     extra = 128 * -(-2 * count // 128)
     named = route_ids[:, :, None] == jnp.arange(count, dtype=jnp.int32)[None, None, :]
     gates = jnp.sum(jnp.where(named, route_weights[:, :, None], 0.0), axis=1)
     coarse = lax.reduce_precision(gates, 8, 7)
     pieces = jnp.concatenate((coarse, gates - coarse), axis=1).astype(jnp.bfloat16)
-    pieces = jnp.pad(pieces, ((0, 0), (0, extra - 2 * count)))
-    extended = jnp.concatenate((normed, pieces), axis=1)
+    return jnp.pad(pieces, ((0, 0), (0, extra - 2 * count)))
+
+
+def dense_experts(
+    extended, mid, expert_gate, expert_up, expert_down, shared_gate, shared_up, shared_down
+):
+    count = lax.axis_size("sp")
+    half = count // 2
+    rows, width = mid.shape
+    extra = extended.shape[1] - width
     fe, sh = expert_gate.shape[2], shared_gate.shape[1]
     vmem, anywhere = pl.BlockSpec(memory_space=pltpu.VMEM), pl.BlockSpec(memory_space=pl.ANY)
     bf16 = jnp.bfloat16
@@ -330,6 +606,22 @@
     tok_rows = query.shape[0]
     kv_local = key_rows.shape[1] // HD
     group_size = query.shape[1] // key_rows.shape[1]
+    count, peers = lax.axis_size("sp"), lax.axis_size("tp")
+    dense = 2 * stream.shape[0] * TOP_K // (count * expert_gate.shape[0]) >= stream.shape[0]
+    even = count % 2 == 0 and count >= 4 and peers % 2 == 0
+    if dense and even and kv_local == 1 and expert_gate.shape[0] == 1:
+        extended, mid = attend(
+            query,
+            key_rows,
+            value_rows,
+            out_weight,
+            stream,
+            norm_gain,
+            gate_pieces(route_ids, route_weights),
+        )
+        return dense_experts(
+            extended, mid, expert_gate, expert_up, expert_down, shared_gate, shared_up, shared_down
+        )
     queries = query.reshape(tok_rows, kv_local, group_size, HD)
     device_pos = lax.axis_index("sp")
     offset = device_pos * tok_rows
@@ -391,19 +683,6 @@
     local_experts = expert_gate.shape[0]
     expert_count = lax.axis_size("sp") * local_experts
     capacity = 2 * own_rows * TOP_K // expert_count
-    if capacity >= own_rows and local_experts == 1 and expert_count % 2 == 0:
-        return dense_experts(
-            normed,
-            mid,
-            route_ids,
-            route_weights,
-            expert_gate,
-            expert_up,
-            expert_down,
-            shared_gate,
-            shared_up,
-            shared_down,
-        )
     slot_count = expert_count * capacity
     flat_ids = route_ids.reshape(-1)
     membership = (flat_ids[:, None] == jnp.arange(expert_count, dtype=jnp.int32)[None, :]).astype(

time: 189 us -> 110 us (0.58)
  waiting for transfers between devices: 60.4 us -> 0 us
  starting transfers between devices: 38.4 us -> 0 us
  Pallas kernels: 63.8 us -> 101 us
  between operations: 13.6 us -> 0.05 us
  matrix products: 4.04 us -> 0 us
    reduce_scatter x1 -> x0, waiting for transfers between devices: 41.7 us -> none  [per_device(): lax.psum_scatter(jnp.dot(heads_out, out_weight, preferred_element_type=jn...]
    ppermute x7 -> x0, starting transfers between devices: 38.4 us -> none  [shifted(): lax.ppermute(value, axis, [(source, source + steps) for source in range(f...]
    pallas_call x0 -> x1, Pallas kernels: none -> 32.8 us  [attend(): pl.pallas_call(functools.partial(attention_kernel, count, peers), out_sha...]
    ppermute x7 -> x0, waiting for transfers between devices: 18.7 us -> none  [shifted(): lax.ppermute(value, axis, [(source, source + steps) for source in range(f...]
    pallas_call x1, Pallas kernels: 63.8 us -> 67.8 us  [dense_experts(): pl.pallas_call(functools.partial(experts_kernel, count), out_shape=jax.Sh...]
    dot_general x5 -> x0, matrix products: 4.04 us -> none  [the longest x1 1.8 us: per_device(): jnp.dot(heads_out, out_weight, preferred_element_type=jnp.float32)]
    unnamed x23 -> x15, local copies, waits for them, and re-layouts: 5.4 us -> 7.29 us
  transfers between devices with their start and end apart: 8 -> 0, of which waited for: 8 -> 0; matrix products, arithmetic and copies ran while one was open for 0% -> 0% of each run, Pallas kernels for 0% -> 0%
where the time goes in v2:
time: 110 us
  Pallas kernels  101 us (92%)
  local copies, waits for them, and re-layouts  7.4 us (7%)
  other arithmetic  1.73 us (2%)
    pallas_call x1, Pallas kernels, dense_experts(): pl.pallas_call(functools.partial(experts_kernel, count), out_shape=jax.Sh...  67.8 us
    pallas_call x1, Pallas kernels, attend(): pl.pallas_call(functools.partial(attention_kernel, count, peers), out_sha...  32.8 us
    unnamed x15, local copies, waits for them, and re-layouts  7.29 us

profile of v2, /device:TPU:0, one launch (start us, length us, event | category | flops | bytes accessed | tf_op | source)
XLA Modules:
  0.0 109.8 jit_solution(5994483245463760099)
XLA Ops:
  0.0 0.0 copy-start
  0.0 0.8 select_reduce_fusion
  0.8 0.1 copy.20
  1.0 0.9 pad_maximum_fusion.kv_ref
  1.9 0.0 copy-start.3
  1.9 1.2 %copy-done.3 = bf16[256,2048]{1,0:T(8,128)(2,1)S(1)} copy-done((bf16[256,2048]{1,0:T(8,128)(2,1)S(1)}, bf16[256,2048]{1,0:T(8,128)(2,1)}, u32[]{:S(2)}) %copy-start.3) | copy-done | bytes 1048600
  3.1 0.0 copy-start.4
  3.1 0.9 copy-done.4
  4.0 0.0 copy-start.5
  4.0 0.9 copy-done.5
  4.9 0.0 copy-start.6
  4.9 0.7 copy-done.6
  5.6 32.8 %shard_map.136 = (bf16[64,2176]{1,0:T(8,128)(2,1)S(1)}, bf16[64,2048]{1,0:T(8,128)(2,1)S(1)}) custom-call(bf16[256,256]{1,0:T(8,128)(2,1)S(1)} %copy-done.5, bf16[256,256]{1,0:T(8,128)(2,1)S(1)} %pad_maximum_fusion.kv_ref, bf16[256,2048]{1,0:T(8,128)(2,1)S(1)} %copy-done.3, bf16[64,2048]{1,0:T(8,128)(2,1)S(1)} %copy-done.4, f32[1,2048]{1,0:T(1,128)S(1)} %bitcast.1, ...), custom_call_target="tpu_custom_call" | custom-call | tf_op jit(solution)/shard_map/pallas_call | solution.py:496
  38.4 0.0 copy-done
  38.5 0.0 copy-start.1
  38.5 1.4 %copy-done.1 = bf16[1,2048,384]{2,1,0:T(8,128)(2,1)S(1)} copy-done((bf16[1,2048,384]{2,1,0:T(8,128)(2,1)S(1)}, bf16[1,2048,384]{2,1,0:T(8,128)(2,1)}, u32[]{:S(2)}) %copy-start.1) | copy-done | bytes 1572888
  39.9 0.0 copy-start.2
  39.9 1.4 %copy-done.2 = bf16[1,384,2048]{2,1,0:T(8,128)(2,1)S(1)} copy-done((bf16[1,384,2048]{2,1,0:T(8,128)(2,1)S(1)}, bf16[1,384,2048]{2,1,0:T(8,128)(2,1)}, u32[]{:S(2)}) %copy-start.2) | copy-done | bytes 1572888
  41.3 67.8 %shard_map.137 = bf16[64,2048]{1,0:T(8,128)(2,1)S(1)} custom-call(bf16[64,2176]{1,0:T(8,128)(2,1)S(1)} %get-tuple-element.7.x_ref, bf16[64,2048]{1,0:T(8,128)(2,1)S(1)} %get-tuple-element.8.mid_ref, bf16[1,2048,384]{2,1,0:T(8,128)(2,1)S(1)} %copy-done, bf16[1,2048,384]{2,1,0:T(8,128)(2,1)S(1)} %copy-done.1, bf16[1,384,2048]{2,1,0:T(8,128)(2,1)S(1)} %copy-done.2, ...), custom_call_target="tpu_custom_call" | custom-call | tf_op jit(solution)/shard_map/pallas_call | solution.py:550
  109.1 0.7 copy.22
  (3 shorter events, 0.0 us)
Async XLA Ops:
  0.0 38.5 %copy-start = (bf16[1,2048,384]{2,1,0:T(8,128)(2,1)S(1)}, bf16[1,2048,384]{2,1,0:T(8,128)(2,1)}, u32[]{:S(2)}) copy-start(bf16[1,2048,384]{2,1,0:T(8,128)(2,1)} %gate_hbm.1) | copy-start | bytes 4718596
  1.9 1.2 %copy-start.3 = (bf16[256,2048]{1,0:T(8,128)(2,1)S(1)}, bf16[256,2048]{1,0:T(8,128)(2,1)}, u32[]{:S(2)}) copy-start(bf16[256,2048]{1,0:T(8,128)(2,1)} %w_hbm.1) | copy-start | bytes 3145732
  3.1 0.9 copy-start.4
  4.0 0.9 copy-start.5
  4.9 0.7 copy-start.6
  38.5 1.4 %copy-start.1 = (bf16[1,2048,384]{2,1,0:T(8,128)(2,1)S(1)}, bf16[1,2048,384]{2,1,0:T(8,128)(2,1)}, u32[]{:S(2)}) copy-start(bf16[1,2048,384]{2,1,0:T(8,128)(2,1)} %up_hbm.1) | copy-start | bytes 4718596
  39.9 1.4 %copy-start.2 = (bf16[1,384,2048]{2,1,0:T(8,128)(2,1)S(1)}, bf16[1,384,2048]{2,1,0:T(8,128)(2,1)}, u32[]{:S(2)}) copy-start(bf16[1,384,2048]{2,1,0:T(8,128)(2,1)} %down_hbm.1) | copy-start | bytes 4718596
